TPU v7x, 32 devices: a whole 2x2x4 slice. The times are simulated.
32 devices in a mesh: grp: 2 (over y), sp: 4 (over z), tp: 4 (over x, core).
Axes of the slice: x: 2, y: 2, z: 4, core: 2. Of those that a mesh axis runs over, the one named last changes fastest.
Arguments:
- stream: bfloat16 [2048, 2048], P(('grp', 'sp'), 'tp'), parts along dimension 0, may hold values from -1.5 to 1.5
- layer_norm_gain: float32 [2, 2048], replicated, may hold values from 0.1 to 1.9
- convolution_in_weight: bfloat16 [2, 2048, 1536], P(None, 'sp', 'tp'), may hold values from -0.125 to 0.125
- gating_in_weight: bfloat16 [2, 2048, 1536], P(None, 'sp', 'tp'), may hold values from -0.125 to 0.125
- output_weight: bfloat16 [2, 1536, 2048], P(None, 'tp', 'sp'), may hold values from -0.15625 to 0.15625
- convolution_kernel_taps: float32 [2, 4, 1536], P(None, None, 'tp'), may hold values from -12 to 12
- recurrent_gate_blocks: bfloat16 [2, 2, 2, 12, 128, 128], P(None, None, None, 'tp'), may hold values from -0.5 to 0.5
- channel_decay_logit: float32 [2, 2, 1536], P(None, None, 'tp')
- position_decay_boost: float32 [2, 2, 2048], P(None, None, ('grp', 'sp')), parts along dimension 2, may hold values from -1.4 to 0, as said below
Outputs:
- new_stream: bfloat16 [2048, 2048], P(('grp', 'sp'), 'tp'), parts along dimension 0
There are 2 independent parts, one for each index of `grp`. A program takes and returns all parts, laid end to end along the dimension named above; an argument that names none is the same for every part. Nothing has to cross between parts.
Inputs may be any that keep to these rules, and one draw needn't show every extreme that they name: `position_decay_boost`: zero at all but a few positions.
All inputs are finite; a program needn't handle non-finite values.
Results may differ from a plain program's by a relative error of at most 0.025.
Values may be sent and summed in bfloat16 or wider, within the bound.
A program may use at most 128 MiB of HBM per device.

v0:
```python
import jax
import jax.numpy as jnp
from jax import lax
from jax.sharding import PartitionSpec as P

EPS = 1e-06
RECURRENT_WIDTH = 8.0


def extended(cells, sides, width):
    for axis, dim in sides:
        count = lax.axis_size(axis)
        ends = count - 1
        head = lax.slice_in_dim(cells, 0, width, axis=dim)
        tail = lax.slice_in_dim(cells, cells.shape[dim] - width, cells.shape[dim], axis=dim)
        cells = jnp.concatenate(
            [
                lax.ppermute(tail, axis, [(i, (i + 1) % count) for i in range(ends)]),
                cells,
                lax.ppermute(head, axis, [((i + 1) % count, i) for i in range(ends)]),
            ],
            axis=dim,
        )
    return cells


def carried_in(part, axis, combine, identity, reverse):
    count = lax.axis_size(axis)
    place = lax.axis_index(axis)
    ahead = count - 1 - place if reverse else place
    gathered = jax.tree.map(lambda a: lax.all_gather(a, axis), part)
    state = jax.tree.map(lambda a, e: jnp.zeros_like(a) + jnp.asarray(e, a.dtype), part, identity)

    def one(step, state):
        source = count - 1 - step if reverse else step
        return combine(
            state, jax.tree.map(lambda a: lax.dynamic_index_in_dim(a, source, 0, False), gathered)
        )

    return lax.fori_loop(0, ahead, one, state)


def rms_norm(values, gain_row):
    floats = values.astype(jnp.float32)
    inverse = lax.rsqrt(jnp.mean(floats * floats, axis=-1, keepdims=True) + EPS)
    return (floats * inverse * gain_row).astype(jnp.bfloat16)


def combine_pairs(earlier, latter):
    return (earlier[0] * latter[0], latter[0] * earlier[1] + latter[1])


def local(
    stream,
    layer_norm_gain,
    convolution_in_weight,
    gating_in_weight,
    output_weight,
    convolution_kernel_taps,
    recurrent_gate_blocks,
    channel_decay_logit,
    position_decay_boost,
):
    tok_rows = stream.shape[0]
    channels = convolution_in_weight.shape[2]
    gate_count = recurrent_gate_blocks.shape[3]
    block_width = recurrent_gate_blocks.shape[4]
    seq_devices = lax.axis_size("sp")
    my_index = lax.axis_index("sp")
    seq_length = tok_rows * seq_devices
    positions = my_index * tok_rows + lax.iota(jnp.int32, tok_rows)
    at_first = (positions == 0)[:, None]
    at_last = (positions == seq_length - 1)[:, None]
    for layer_index in range(convolution_in_weight.shape[0]):
        features = lax.all_gather(stream, "tp", axis=1, tiled=True)
        normed = rms_norm(features, layer_norm_gain[layer_index])
        acc_x = jnp.dot(
            normed,
            lax.all_gather(convolution_in_weight[layer_index], "sp", axis=0, tiled=True),
            preferred_element_type=jnp.float32,
        )
        acc_y = jnp.dot(
            normed,
            lax.all_gather(gating_in_weight[layer_index], "sp", axis=0, tiled=True),
            preferred_element_type=jnp.float32,
        )
        proj_x = acc_x.astype(jnp.bfloat16)
        proj_y = acc_y.astype(jnp.bfloat16)
        padded = extended(proj_x, (("sp", 0),), 2).astype(jnp.float32)
        taps_now = convolution_kernel_taps[layer_index]
        conv_mixed = (
            taps_now[0] * padded[1 : tok_rows + 1]
            + taps_now[1] * padded[2 : tok_rows + 2]
            + taps_now[2] * padded[3 : tok_rows + 3]
            + taps_now[3] * padded[4 : tok_rows + 4]
        )
        convolution_output = conv_mixed.astype(jnp.bfloat16)
        conv_float = convolution_output.astype(jnp.float32)
        grouped = convolution_output.reshape(tok_rows, gate_count, block_width)
        results = []
        for scan_direction in range(2):
            gate_matrix_pair = recurrent_gate_blocks[layer_index, scan_direction]
            recurrent_branch = jax.nn.sigmoid(
                jnp.einsum(
                    "tnc,ncd->tnd", grouped, gate_matrix_pair[0], preferred_element_type=jnp.float32
                ).reshape(tok_rows, channels)
            )
            input_gate = jax.nn.sigmoid(
                jnp.einsum(
                    "tnc,ncd->tnd", grouped, gate_matrix_pair[1], preferred_element_type=jnp.float32
                ).reshape(tok_rows, channels)
            )
            decay_logarithm = (
                -RECURRENT_WIDTH
                * jax.nn.softplus(-channel_decay_logit[layer_index, scan_direction])
                * recurrent_branch
                + position_decay_boost[layer_index, scan_direction][:, None]
            )
            is_start = at_first if scan_direction == 0 else at_last
            multiplier = jnp.where(is_start, 1.0, jnp.sqrt(-jnp.expm1(2.0 * decay_logarithm)))
            driven = multiplier * input_gate * conv_float
            results.append(
                lax.associative_scan(
                    combine_pairs,
                    (jnp.exp(decay_logarithm), driven),
                    reverse=scan_direction == 1,
                    axis=0,
                )
            )
        cum_fwd, local_fwd = results[0]
        cum_bwd, local_bwd = results[1]
        identity = (jnp.ones((1, channels), jnp.float32), jnp.zeros((1, channels), jnp.float32))
        enter_fwd = carried_in(
            (cum_fwd[-1:], local_fwd[-1:]), "sp", combine_pairs, identity, False
        )[1]
        enter_bwd = carried_in((cum_bwd[:1], local_bwd[:1]), "sp", combine_pairs, identity, True)[1]
        state_sum = local_fwd + cum_fwd * enter_fwd + local_bwd + cum_bwd * enter_bwd
        gated = (state_sum * jax.nn.gelu(proj_y.astype(jnp.float32))).astype(jnp.bfloat16)
        partials = jnp.dot(
            gated,
            lax.all_gather(output_weight[layer_index], "sp", axis=1, tiled=True),
            preferred_element_type=jnp.float32,
        ).astype(jnp.bfloat16)
        branch_sum = lax.psum_scatter(
            partials.astype(jnp.float32).astype(jnp.bfloat16), "tp", scatter_dimension=1, tiled=True
        ).astype(jnp.float32)
        stream = (stream.astype(jnp.float32) + branch_sum).astype(jnp.bfloat16)
    return stream


def solution(mesh):
    return jax.shard_map(
        local,
        mesh=mesh,
        in_specs=(
            P(("grp", "sp"), "tp"),
            P(),
            P(None, "sp", "tp"),
            P(None, "sp", "tp"),
            P(None, "tp", "sp"),
            P(None, None, "tp"),
            P(None, None, None, "tp", None, None),
            P(None, None, "tp"),
            P(None, None, ("grp", "sp")),
        ),
        out_specs=P(("grp", "sp"), "tp"),
        check_vma=False,
    )
```

profile of v0, /device:TPU:0, one launch (start us, length us, event | category | flops | bytes accessed | tf_op | source)
XLA Modules:
  0.0 358.1 jit_solution(14976978191996592059)
XLA Ops:
  6.5 0.7 all-gather.31.cloned.1.call-update
  7.3 2.1 fusion.206
  9.5 1.0 fusion.207
  10.7 0.9 fusion.208
  11.7 0.6 fusion.211
  12.3 0.7 slice_reduce_fusion.3
  13.0 0.6 negate_reduce_fusion.1
  13.6 0.5 fusion.196
  14.1 0.6 fusion.216
  14.7 0.6 fusion.176
  15.3 13.0 %all-gather.31.cloned.1.call-done = bf16[256,2048]{1,0:T(8,128)(2,1)} async-done(((bf16[256,512]{1,0:T(8,128)(2,1)}), bf16[256,2048]{1,0:T(8,128)(2,1)}) %all-gather.31.cloned.1.call-update) | async-done | bytes 1048592 | tf_op jit(solution)/shard_map/all_gather | solution.py:75
  28.3 1.5 fusion
  29.9 37.1 %all-gather.35.cloned.1.call-done = bf16[1,2048,384]{2,1,0:T(8,128)(2,1)} async-done(((bf16[1,512,384]{2,1,0:T(8,128)(2,1)}), bf16[1,2048,384]{2,1,0:T(8,128)(2,1)}) %all-gather.35.cloned.1.call-update) | async-done | bytes 1572880 | tf_op jit(solution)/shard_map/all_gather | solution.py:79
  67.0 2.5 fusion.40
  69.5 2.6 collective-permute-start
  72.1 1.3 collective-permute-start.1
  73.5 4.2 %collective-permute-done.1 = bf16[2,384]{1,0:T(2,128)(2,1)S(1)} collective-permute-done((bf16[2,384]{1,0:T(2,128)(2,1)S(1)}, bf16[2,384]{1,0:T(2,128)(2,1)S(1)}, u32[]{:S(2)}, u32[]{:S(2)}) %collective-permute-start.1) | collective-permute-done | bytes 1568 | tf_op jit(solution)/shard_map/ppermute | solution.py:20
  80.0 1.6 convert_multiply_fusion.7
  87.3 12.3 %all-gather.15 = f32[4,1,384]{2,1,0:T(1,128)S(1)} all-gather(f32[1,1,384]{2,1,0:T(1,128)S(1)} %add_bitcast_fusion.6), channel_id=4, replica_groups=mesh['grp'=2,'sp'=4,'tp'=4] {'sp'}, dimensions={0}, use_global_device_ids=true | all-gather | bytes 7680 | tf_op jit(solution)/shard_map/all_gather | solution.py:31
  99.7 11.9 %all-gather.14 = f32[4,1,384]{2,1,0:T(1,128)S(1)} all-gather(f32[1,1,384]{2,1,0:T(1,128)S(1)} %add_bitcast_fusion.7), channel_id=3, replica_groups=mesh['grp'=2,'sp'=4,'tp'=4] {'sp'}, dimensions={0}, use_global_device_ids=true | all-gather | bytes 7680 | tf_op jit(solution)/shard_map/all_gather | solution.py:31
  112.4 0.6 slice.1577
  112.9 0.6 slice.1603
  113.8 0.5 slice.1576
  114.8 0.7 pad_maximum_fusion.10
  116.5 1.6 pad.454
  118.1 0.8 add.988
  118.9 1.9 add.997
  120.8 0.7 add_bitcast_fusion.4
  121.5 12.5 %all-gather.17 = f32[4,1,384]{2,1,0:T(1,128)S(1)} all-gather(f32[1,1,384]{2,1,0:T(1,128)S(1)} %add_bitcast_fusion.4), channel_id=6, replica_groups=mesh['grp'=2,'sp'=4,'tp'=4] {'sp'}, dimensions={0}, use_global_device_ids=true | all-gather | bytes 7680 | tf_op jit(solution)/shard_map/all_gather | solution.py:31
  134.0 0.7 add_bitcast_fusion.5
  134.7 12.1 %all-gather.16 = f32[4,1,384]{2,1,0:T(1,128)S(1)} all-gather(f32[1,1,384]{2,1,0:T(1,128)S(1)} %add_bitcast_fusion.5), channel_id=5, replica_groups=mesh['grp'=2,'sp'=4,'tp'=4] {'sp'}, dimensions={0}, use_global_device_ids=true | all-gather | bytes 7680 | tf_op jit(solution)/shard_map/all_gather | solution.py:31
  146.9 2.6 rev.16
  149.5 2.6 rev.17
  152.2 4.4 %convolution_convert_fusion.1 = bf16[256,2048]{1,0:T(8,128)(2,1)} fusion(bf16[1,384,2048]{2,1,0:T(8,128)(2,1)} %all-gather.39.cloned.1.call-done, bf16[1,2048,384]{2,1,0:T(8,128)(2,1)} %all-gather.37.cloned.1.call-done, f32[256,384]{1,0:T(8,128)S(1)} %rev.17, f32[256,384]{1,0:T(8,128)S(1)} %rev.16, f32[256,384]{1,0:T(8,128)S(1)} %pad.422, ...), kind=kOutput, calls=%fused_computation.13 | convolution fusion | flops 809795584 | bytes 7614464 | tf_op jit(solution)/shard_map/dot_general | solution.py:139
  156.9 22.8 %reduce-scatter.3.cloned.1.call-done = bf16[256,512]{1,0:T(8,128)(2,1)} async-done(((bf16[256,2048]{1,0:T(8,128)(2,1)}), bf16[256,512]{1,0:T(8,128)(2,1)}) %reduce-scatter.3.cloned.1.call-update) | async-done | bytes 262160 | tf_op jit(solution)/shard_map/reduce_scatter | solution.py:144
  179.6 1.8 add_convert_fusion.1
  181.5 0.7 all-gather.41.cloned.1.call-update
  182.3 0.7 all-gather.43.cloned.1.call-update
  183.0 0.7 all-gather.45.cloned.1.call-update
  183.8 0.6 fusion.178
  184.4 13.9 %all-gather.33.cloned.1.call-done = bf16[256,2048]{1,0:T(8,128)(2,1)} async-done(((bf16[256,512]{1,0:T(8,128)(2,1)}), bf16[256,2048]{1,0:T(8,128)(2,1)}) %all-gather.33.cloned.1.call-update) | async-done | bytes 1048592 | tf_op jit(solution)/shard_map/all_gather | solution.py:75
  198.3 1.5 fusion.3
  199.8 37.1 %all-gather.41.cloned.1.call-done = bf16[1,2048,384]{2,1,0:T(8,128)(2,1)} async-done(((bf16[1,512,384]{2,1,0:T(8,128)(2,1)}), bf16[1,2048,384]{2,1,0:T(8,128)(2,1)}) %all-gather.41.cloned.1.call-update) | async-done | bytes 1572880 | tf_op jit(solution)/shard_map/all_gather | solution.py:79
  236.9 2.5 fusion.49
  239.5 2.6 collective-permute-start.2
  242.1 1.3 collective-permute-start.3
  243.4 4.2 %collective-permute-done.3 = bf16[2,384]{1,0:T(2,128)(2,1)S(1)} collective-permute-done((bf16[2,384]{1,0:T(2,128)(2,1)S(1)}, bf16[2,384]{1,0:T(2,128)(2,1)S(1)}, u32[]{:S(2)}, u32[]{:S(2)}) %collective-permute-start.3) | collective-permute-done | bytes 1568 | tf_op jit(solution)/shard_map/ppermute | solution.py:20
  250.0 1.6 convert_multiply_fusion.5
  257.2 12.3 %all-gather.19 = f32[4,1,384]{2,1,0:T(1,128)S(1)} all-gather(f32[1,1,384]{2,1,0:T(1,128)S(1)} %add_bitcast_fusion.2), channel_id=11, replica_groups=mesh['grp'=2,'sp'=4,'tp'=4] {'sp'}, dimensions={0}, use_global_device_ids=true | all-gather | bytes 7680 | tf_op jit(solution)/shard_map/all_gather | solution.py:31
  269.7 11.9 %all-gather.18 = f32[4,1,384]{2,1,0:T(1,128)S(1)} all-gather(f32[1,1,384]{2,1,0:T(1,128)S(1)} %add_bitcast_fusion.3), channel_id=10, replica_groups=mesh['grp'=2,'sp'=4,'tp'=4] {'sp'}, dimensions={0}, use_global_device_ids=true | all-gather | bytes 7680 | tf_op jit(solution)/shard_map/all_gather | solution.py:31
  282.3 0.6 slice.1687
  283.7 0.7 pad_maximum_fusion.14
  284.9 1.6 pad.518
  286.5 0.8 add.1076
  287.4 1.9 add.1085
  289.2 0.7 add_bitcast_fusion
  289.9 12.4 %all-gather.21 = f32[4,1,384]{2,1,0:T(1,128)S(1)} all-gather(f32[1,1,384]{2,1,0:T(1,128)S(1)} %add_bitcast_fusion), channel_id=13, replica_groups=mesh['grp'=2,'sp'=4,'tp'=4] {'sp'}, dimensions={0}, use_global_device_ids=true | all-gather | bytes 7680 | tf_op jit(solution)/shard_map/all_gather | solution.py:31
  302.3 0.7 add_bitcast_fusion.1
  303.0 12.1 %all-gather.20 = f32[4,1,384]{2,1,0:T(1,128)S(1)} all-gather(f32[1,1,384]{2,1,0:T(1,128)S(1)} %add_bitcast_fusion.1), channel_id=12, replica_groups=mesh['grp'=2,'sp'=4,'tp'=4] {'sp'}, dimensions={0}, use_global_device_ids=true | all-gather | bytes 7680 | tf_op jit(solution)/shard_map/all_gather | solution.py:31
  315.2 2.6 rev.18
  317.8 3.9 %rev.19 = f32[256,384]{1,0:T(8,128)} reverse(f32[256,384]{1,0:T(8,128)} %add.1085), dimensions={0} | reverse | bytes 786432 | tf_op jit(solution)/shard_map/rev | solution.py:123
  321.7 4.6 %convolution_convert_fusion = bf16[256,2048]{1,0:T(8,128)(2,1)} fusion(bf16[1,384,2048]{2,1,0:T(8,128)(2,1)} %all-gather.45.cloned.1.call-done, bf16[1,2048,384]{2,1,0:T(8,128)(2,1)} %all-gather.43.cloned.1.call-done, f32[256,384]{1,0:T(8,128)} %rev.19, f32[256,384]{1,0:T(8,128)S(1)} %rev.18, f32[256,384]{1,0:T(8,128)S(1)} %pad.486, ...), kind=kOutput, calls=%fused_computation.12 | convolution fusion | flops 809795584 | bytes 7614464 | tf_op jit(solution)/shard_map/dot_general | solution.py:139
  326.3 23.2 %reduce-scatter.5.cloned.1.call-done = bf16[256,512]{1,0:T(8,128)(2,1)} async-done(((bf16[256,2048]{1,0:T(8,128)(2,1)}), bf16[256,512]{1,0:T(8,128)(2,1)}) %reduce-scatter.5.cloned.1.call-update) | async-done | bytes 262160 | tf_op jit(solution)/shard_map/reduce_scatter | solution.py:144
  349.5 1.7 add_convert_fusion
  (630 shorter events, 19.1 us)
Async XLA Ops:
  6.5 2.9 copy-start.5
  6.5 21.8 %all-gather.31.cloned.1.call-start = ((), (), s32[]{:S(2)}) async-start(), calls=%async_computation.2 | async-start | bytes 1310720 | tf_op jit(solution)/shard_map/all_gather | solution.py:75
  7.3 59.7 %all-gather.35.cloned.1.call-start = ((), (), s32[]{:S(2)}) async-start(), calls=%async_computation.6 | async-start | bytes 1966080 | tf_op jit(solution)/shard_map/all_gather | solution.py:79
  9.4 1.3 copy-start.6
  9.4 142.7 %all-gather.37.cloned.1.call-start = ((), (), s32[]{:S(2)}) async-start(), calls=%async_computation.7 | async-start | bytes 1966080 | tf_op jit(solution)/shard_map/all_gather | solution.py:84
  10.4 1.2 copy-start.18
  10.4 1.8 copy-start.19
  10.4 2.5 copy-start.24
  10.4 3.7 %copy-start.29 = (f32[2,2,256]{2,1,0:T(2,128)S(1)}, f32[2,2,256]{2,1,0:T(2,128)}, u32[]{:S(2)}) copy-start(f32[2,2,256]{2,1,0:T(2,128)} %param.25) | copy-start | bytes 12292
  10.5 141.7 %all-gather.39.cloned.1.call-start = ((), (), s32[]{:S(2)}) async-start(), calls=%async_computation.8 | async-start | bytes 1966080 | tf_op jit(solution)/shard_map/all_gather | solution.py:141
  11.6 168.0 %reduce-scatter.3.cloned.1.call-start = ((), (), s32[]{:S(2)}) async-start(), calls=%async_computation.3 | async-start | bytes 1310720 | tf_op jit(solution)/shard_map/reduce_scatter | solution.py:144
  12.3 57.2 %copy-start.9 = (f32[1,2048]{1,0:T(1,128)}, f32[1,2048]{1,0:T(1,128)S(1)}, u32[]{:S(2)}) copy-start(f32[1,2048]{1,0:T(1,128)S(1)} %get-tuple-element.404) | copy-start | bytes 24580
  12.9 64.7 %copy-start.14 = (f32[384]{0:T(512)}, f32[384]{0:T(512)S(1)}, u32[]{:S(2)}) copy-start(f32[384]{0:T(512)S(1)} %get-tuple-element.267) | copy-start | bytes 4612
  12.9 64.7 %copy-start.15 = (f32[384]{0:T(512)}, f32[384]{0:T(512)S(1)}, u32[]{:S(2)}) copy-start(f32[384]{0:T(512)S(1)} %get-tuple-element.268) | copy-start | bytes 4612
  12.9 64.7 %copy-start.16 = (f32[384]{0:T(512)}, f32[384]{0:T(512)S(1)}, u32[]{:S(2)}) copy-start(f32[384]{0:T(512)S(1)} %get-tuple-element.269) | copy-start | bytes 4612
  12.9 64.8 %copy-start.17 = (f32[384]{0:T(512)}, f32[384]{0:T(512)S(1)}, u32[]{:S(2)}) copy-start(f32[384]{0:T(512)S(1)} %get-tuple-element.270) | copy-start | bytes 4612
  29.9 39.6 %copy-start.27 = (f32[256]{0:T(256)}, f32[256]{0:T(256)S(1)}, u32[]{:S(2)}) copy-start(f32[256]{0:T(256)S(1)} %add_rsqrt_fusion.1) | copy-start | bytes 3076
  69.5 8.6 %copy-start.30 = (bf16[2,2,2,3,128,128]{5,4,3,2,1,0:T(8,128)(2,1)S(1)}, bf16[2,2,2,3,128,128]{5,4,3,2,1,0:T(8,128)(2,1)}, u32[]{:S(2)}) copy-start(bf16[2,2,2,3,128,128]{5,4,3,2,1,0:T(8,128)(2,1)} %param.23) | copy-start | bytes 2359300
  69.5 3.9 %collective-permute-start = (bf16[2,384]{1,0:T(2,128)(2,1)S(1)}, bf16[2,384]{1,0:T(2,128)(2,1)S(1)}, u32[]{:S(2)}, u32[]{:S(2)}) collective-permute-start(bf16[2,384]{1,0:T(2,128)(2,1)S(1)} %get-tuple-element.353), channel_id=1, source_target_pairs={{0,4},{4,8},{8,12},{1,5},{5,9},{9,13},{2,6},{6,10},{10,14},{3,7},{... | collective-permute-start | bytes 4616 | tf_op jit(solution)/shard_map/ppermute | solution.py:18
  72.1 5.5 %collective-permute-start.1 = (bf16[2,384]{1,0:T(2,128)(2,1)S(1)}, bf16[2,384]{1,0:T(2,128)(2,1)S(1)}, u32[]{:S(2)}, u32[]{:S(2)}) collective-permute-start(bf16[2,384]{1,0:T(2,128)(2,1)S(1)} %get-tuple-element.354), channel_id=1, source_target_pairs={{4,0},{8,4},{12,8},{5,1},{9,5},{13,9},{6,2},{10,6},{14,10},{7,3},{... | collective-permute-start | bytes 4616 | tf_op jit(solution)/shard_map/ppermute | solution.py:20
  114.7 0.9 copy-start.23
  115.7 0.6 copy-start.22
  116.4 1.7 copy-start.3
  118.9 33.3 %copy-start = (bf16[256,2048]{1,0:T(8,128)(2,1)S(1)}, bf16[256,2048]{1,0:T(8,128)(2,1)}, u32[]{:S(2)}) copy-start(bf16[256,2048]{1,0:T(8,128)(2,1)} %all-gather.31.cloned.1.call-done) | copy-start | bytes 3145732
  118.9 33.3 %copy-start.10 = (f32[1,2048]{1,0:T(1,128)S(1)}, f32[1,2048]{1,0:T(1,128)}, u32[]{:S(2)}) copy-start(f32[1,2048]{1,0:T(1,128)} %copy-done.9) | copy-start | bytes 24580
  118.9 33.3 %copy-start.28 = (f32[256]{0:T(256)S(1)}, f32[256]{0:T(256)}, u32[]{:S(2)}) copy-start(f32[256]{0:T(256)} %copy-done.27) | copy-start | bytes 3076
  156.6 27.1 %copy-start.20 = (f32[384]{0:T(512)S(1)}, f32[384]{0:T(512)}, u32[]{:S(2)}) copy-start(f32[384]{0:T(512)} %get-tuple-element.273) | copy-start | bytes 4612
  156.6 27.2 %copy-start.21 = (f32[384]{0:T(512)S(1)}, f32[384]{0:T(512)}, u32[]{:S(2)}) copy-start(f32[384]{0:T(512)} %get-tuple-element.276) | copy-start | bytes 4612
  156.6 80.3 %copy-start.7 = (f32[1,2048]{1,0:T(1,128)S(1)}, f32[1,2048]{1,0:T(1,128)}, u32[]{:S(2)}) copy-start(f32[1,2048]{1,0:T(1,128)} %get-tuple-element.403) | copy-start | bytes 24580
  156.6 41.7 %all-gather.33.cloned.1.call-start = ((), (), s32[]{:S(2)}) async-start(), calls=%async_computation.4 | async-start | bytes 1310720 | tf_op jit(solution)/shard_map/all_gather | solution.py:75
  181.5 55.5 %all-gather.41.cloned.1.call-start = ((), (), s32[]{:S(2)}) async-start(), calls=%async_computation.9 | async-start | bytes 1966080 | tf_op jit(solution)/shard_map/all_gather | solution.py:79
  182.2 139.5 %all-gather.43.cloned.1.call-start = ((), (), s32[]{:S(2)}) async-start(), calls=%async_computation.10 | async-start | bytes 1966080 | tf_op jit(solution)/shard_map/all_gather | solution.py:84
  183.0 138.7 %all-gather.45.cloned.1.call-start = ((), (), s32[]{:S(2)}) async-start(), calls=%async_computation.11 | async-start | bytes 1966080 | tf_op jit(solution)/shard_map/all_gather | solution.py:141
  183.7 165.8 %reduce-scatter.5.cloned.1.call-start = ((), (), s32[]{:S(2)}) async-start(), calls=%async_computation.5 | async-start | bytes 1310720 | tf_op jit(solution)/shard_map/reduce_scatter | solution.py:144
  199.8 39.6 %copy-start.25 = (f32[256]{0:T(256)}, f32[256]{0:T(256)S(1)}, u32[]{:S(2)}) copy-start(f32[256]{0:T(256)S(1)} %add_rsqrt_fusion) | copy-start | bytes 3076
  236.9 10.7 %copy-start.11 = (f32[384]{0:T(512)S(1)}, f32[384]{0:T(512)}, u32[]{:S(2)}) copy-start(f32[384]{0:T(512)} %get-tuple-element.266) | copy-start | bytes 4612
  236.9 10.7 %copy-start.12 = (f32[384]{0:T(512)S(1)}, f32[384]{0:T(512)}, u32[]{:S(2)}) copy-start(f32[384]{0:T(512)} %get-tuple-element.271) | copy-start | bytes 4612
  236.9 10.7 %copy-start.13 = (f32[384]{0:T(512)S(1)}, f32[384]{0:T(512)}, u32[]{:S(2)}) copy-start(f32[384]{0:T(512)} %get-tuple-element.272) | copy-start | bytes 4612
  239.4 8.6 %copy-start.31 = (bf16[2,2,2,3,128,128]{5,4,3,2,1,0:T(8,128)(2,1)S(1)}, bf16[2,2,2,3,128,128]{5,4,3,2,1,0:T(8,128)(2,1)}, u32[]{:S(2)}) copy-start(bf16[2,2,2,3,128,128]{5,4,3,2,1,0:T(8,128)(2,1)} %param.23) | copy-start | bytes 2359300
  239.5 3.9 %collective-permute-start.2 = (bf16[2,384]{1,0:T(2,128)(2,1)S(1)}, bf16[2,384]{1,0:T(2,128)(2,1)S(1)}, u32[]{:S(2)}, u32[]{:S(2)}) collective-permute-start(bf16[2,384]{1,0:T(2,128)(2,1)S(1)} %get-tuple-element.341), channel_id=1, source_target_pairs={{0,4},{4,8},{8,12},{1,5},{5,9},{9,13},{2,6},{6,10},{10,14},{3,7},{... | collective-permute-start | bytes 4616 | tf_op jit(solution)/shard_map/ppermute | solution.py:18
  242.1 5.5 %collective-permute-start.3 = (bf16[2,384]{1,0:T(2,128)(2,1)S(1)}, bf16[2,384]{1,0:T(2,128)(2,1)S(1)}, u32[]{:S(2)}, u32[]{:S(2)}) collective-permute-start(bf16[2,384]{1,0:T(2,128)(2,1)S(1)} %get-tuple-element.342), channel_id=1, source_target_pairs={{4,0},{8,4},{12,8},{5,1},{9,5},{13,9},{6,2},{10,6},{14,10},{7,3},{... | collective-permute-start | bytes 4616 | tf_op jit(solution)/shard_map/ppermute | solution.py:20
  284.8 1.7 copy-start.4
  287.3 34.3 %copy-start.1 = (bf16[256,2048]{1,0:T(8,128)(2,1)S(1)}, bf16[256,2048]{1,0:T(8,128)(2,1)}, u32[]{:S(2)}) copy-start(bf16[256,2048]{1,0:T(8,128)(2,1)} %all-gather.33.cloned.1.call-done) | copy-start | bytes 3145732
  287.4 34.3 %copy-start.8 = (f32[1,2048]{1,0:T(1,128)S(1)}, f32[1,2048]{1,0:T(1,128)}, u32[]{:S(2)}) copy-start(f32[1,2048]{1,0:T(1,128)} %get-tuple-element.403) | copy-start | bytes 24580
  287.4 34.3 %copy-start.26 = (f32[256]{0:T(256)S(1)}, f32[256]{0:T(256)}, u32[]{:S(2)}) copy-start(f32[256]{0:T(256)} %copy-done.25) | copy-start | bytes 3076
  321.7 27.8 %copy-start.2 = (bf16[256,512]{1,0:T(8,128)(2,1)S(1)}, bf16[256,512]{1,0:T(8,128)(2,1)}, u32[]{:S(2)}) copy-start(bf16[256,512]{1,0:T(8,128)(2,1)} %add_convert_fusion.1) | copy-start | bytes 786436
Sparse Core Ops, SparseCore 0:
  8.9 19.4 all-gather.30
  29.9 37.0 all-gather.34
  68.5 36.0 all-gather.36
  106.0 36.0 all-gather.38
  156.7 22.8 reduce-scatter.2
  181.6 16.6 all-gather.32
  199.9 37.0 all-gather.40
  238.5 36.0 all-gather.42
  276.1 36.0 all-gather.44
  326.4 23.0 reduce-scatter.4
where the time goes:
time: 360 us; the launch traced here: 358 us
  waiting for transfers between devices  158 us (44%)
  blocking collectives  97.5 us (27%)
  local copies, waits for them, and re-layouts  35.6 us (10%)
  other arithmetic  24.8 us (7%)
  between operations  16.9 us (5%)
  matrix products  16.4 us (5%)
  starting transfers between devices  8.37 us (2%)
    all_gather x8, blocking collectives, carried_in(): gathered = jax.tree.map(lambda a: lax.all_gather(a, axis), part)  97.5 us
    all_gather x2, waiting for transfers between devices, local(): lax.all_gather(convolution_in_weight[layer_index], 'sp', axis=0, tiled=True)  74.2 us
    reduce_scatter x2, waiting for transfers between devices, local(): lax.psum_scatter(partials.astype(jnp.float32).astype(jnp.bfloat16), 'tp',...  46 us
    all_gather x2, waiting for transfers between devices, local(): features = lax.all_gather(stream, 'tp', axis=1, tiled=True)  27 us
    rev x4, local copies, waits for them, and re-layouts, local(): lax.associative_scan(combine_pairs, (jnp.exp(decay_logarithm), driven), r...  11.6 us
    slice x220, local copies, waits for them, and re-layouts, local(): lax.associative_scan(combine_pairs, (jnp.exp(decay_logarithm), driven), r...  10.5 us
    dot_general x2, matrix products, local(): jnp.dot(gated, lax.all_gather(output_weight[layer_index], 'sp', axis=1, t...  8.97 us
    ppermute x2, waiting for transfers between devices, extended(): lax.ppermute(head, axis, [((i + 1) % count, i) for i in range(ends)])  8.32 us
  transfers between devices with their start and end apart: 14, of which 8 were waited for; matrix products, arithmetic and copies ran while one was open for 18% of the time, Pallas kernels for 0%

commit v1 on v0

--- a/solution.py
+++ b/solution.py
@@ -24,20 +24,16 @@
     return cells
 
 
-def carried_in(part, axis, combine, identity, reverse):
-    count = lax.axis_size(axis)
-    place = lax.axis_index(axis)
-    ahead = count - 1 - place if reverse else place
-    gathered = jax.tree.map(lambda a: lax.all_gather(a, axis), part)
-    state = jax.tree.map(lambda a, e: jnp.zeros_like(a) + jnp.asarray(e, a.dtype), part, identity)
-
-    def one(step, state):
-        source = count - 1 - step if reverse else step
-        return combine(
-            state, jax.tree.map(lambda a: lax.dynamic_index_in_dim(a, source, 0, False), gathered)
+def entering(ends, place, count):
+    forward = jnp.zeros_like(ends[0, :1])
+    backward = forward
+    for step in range(count - 1):
+        forward = jnp.where(step < place, ends[step, 0:1] * forward + ends[step, 1:2], forward)
+        source = count - 1 - step
+        backward = jnp.where(
+            source > place, ends[source, 2:3] * backward + ends[source, 3:4], backward
         )
-
-    return lax.fori_loop(0, ahead, one, state)
+    return forward, backward
 
 
 def rms_norm(values, gain_row):
@@ -129,11 +125,8 @@
             )
         cum_fwd, local_fwd = results[0]
         cum_bwd, local_bwd = results[1]
-        identity = (jnp.ones((1, channels), jnp.float32), jnp.zeros((1, channels), jnp.float32))
-        enter_fwd = carried_in(
-            (cum_fwd[-1:], local_fwd[-1:]), "sp", combine_pairs, identity, False
-        )[1]
-        enter_bwd = carried_in((cum_bwd[:1], local_bwd[:1]), "sp", combine_pairs, identity, True)[1]
+        ends = jnp.concatenate([cum_fwd[-1:], local_fwd[-1:], cum_bwd[:1], local_bwd[:1]], axis=0)
+        enter_fwd, enter_bwd = entering(lax.all_gather(ends, "sp"), my_index, seq_devices)
         state_sum = local_fwd + cum_fwd * enter_fwd + local_bwd + cum_bwd * enter_bwd
         gated = (state_sum * jax.nn.gelu(proj_y.astype(jnp.float32))).astype(jnp.bfloat16)
         partials = jnp.dot(

time: 360 us -> 341 us (0.947)
  blocking collectives: 97.5 us -> 27 us
  waiting for transfers between devices: 158 us -> 201 us
  local copies, waits for them, and re-layouts: 35.6 us -> 42.5 us
    all_gather x8 -> x2, blocking collectives: 97.5 us -> 27 us  [local(): lax.all_gather(ends, 'sp')]
    all_gather x2, waiting for transfers between devices: 0.02 us -> 40.9 us  [local(): lax.all_gather(output_weight[layer_index], 'sp', axis=1, tiled=True)]
    add x60 -> x68, other arithmetic: 5.93 us -> 10.5 us  [local(): lax.associative_scan(combine_pairs, (jnp.exp(decay_logarithm), driven), r...]
    rev x4, local copies, waits for them, and re-layouts: 11.6 us -> 15.6 us  [local(): lax.associative_scan(combine_pairs, (jnp.exp(decay_logarithm), driven), r...]
  transfers between devices with their start and end apart: 14 -> 14, of which waited for: 8 -> 10; matrix products, arithmetic and copies ran while one was open for 18% -> 21% of each run, Pallas kernels for 0% -> 0%
where the time goes in v1:
time: 341 us; the launch traced here: 340 us
  waiting for transfers between devices  201 us (59%)
  local copies, waits for them, and re-layouts  42.5 us (12%)
  other arithmetic  27.8 us (8%)
  blocking collectives  27 us (8%)
  between operations  16.9 us (5%)
  matrix products  16.7 us (5%)
  starting transfers between devices  8.38 us (2%)
    all_gather x2, waiting for transfers between devices, local(): lax.all_gather(convolution_in_weight[layer_index], 'sp', axis=0, tiled=True)  74.2 us
    reduce_scatter x2, waiting for transfers between devices, local(): lax.psum_scatter(partials.astype(jnp.float32).astype(jnp.bfloat16), 'tp',...  47.5 us
    all_gather x2, waiting for transfers between devices, local(): lax.all_gather(output_weight[layer_index], 'sp', axis=1, tiled=True)  40.9 us
    all_gather x2, waiting for transfers between devices, local(): features = lax.all_gather(stream, 'tp', axis=1, tiled=True)  28.1 us
    all_gather x2, blocking collectives, local(): lax.all_gather(ends, 'sp')  27 us
    rev x4, local copies, waits for them, and re-layouts, local(): lax.associative_scan(combine_pairs, (jnp.exp(decay_logarithm), driven), r...  15.6 us
    add x68, other arithmetic, local(): lax.associative_scan(combine_pairs, (jnp.exp(decay_logarithm), driven), r...  10.5 us
    dot_general x2, matrix products, local(): jnp.dot(gated, lax.all_gather(output_weight[layer_index], 'sp', axis=1, t...  9.31 us
  transfers between devices with their start and end apart: 14, of which 10 were waited for; matrix products, arithmetic and copies ran while one was open for 21% of the time, Pallas kernels for 0%

profile of v1, /device:TPU:0, one launch (start us, length us, event | category | flops | bytes accessed | tf_op | source)
XLA Modules:
  0.0 339.8 jit_solution(17607182247680082666)
XLA Ops:
  6.5 0.7 all-gather.19.cloned.1.call-update
  7.3 2.1 fusion.210
  9.5 1.0 fusion.211
  10.7 1.0 fusion.212
  12.4 0.6 slice_reduce_fusion.19
  14.2 0.6 fusion.176
  14.8 13.5 %all-gather.19.cloned.1.call-done = bf16[256,2048]{1,0:T(8,128)(2,1)} async-done(((bf16[256,512]{1,0:T(8,128)(2,1)}), bf16[256,2048]{1,0:T(8,128)(2,1)}) %all-gather.19.cloned.1.call-update) | async-done | bytes 1048592 | tf_op jit(solution)/shard_map/all_gather | solution.py:71
  28.3 1.5 fusion
  29.9 37.1 %all-gather.23.cloned.1.call-done = bf16[1,2048,384]{2,1,0:T(8,128)(2,1)} async-done(((bf16[1,512,384]{2,1,0:T(8,128)(2,1)}), bf16[1,2048,384]{2,1,0:T(8,128)(2,1)}) %all-gather.23.cloned.1.call-update) | async-done | bytes 1572880 | tf_op jit(solution)/shard_map/all_gather | solution.py:75
  67.0 2.5 fusion.40
  69.5 2.6 collective-permute-start
  72.1 1.3 collective-permute-start.1
  74.0 3.6 %collective-permute-done.1 = bf16[2,384]{1,0:T(2,128)(2,1)S(1)} collective-permute-done((bf16[2,384]{1,0:T(2,128)(2,1)S(1)}, bf16[2,384]{1,0:T(2,128)(2,1)S(1)}, u32[]{:S(2)}, u32[]{:S(2)}) %collective-permute-start.1) | collective-permute-done | bytes 1568 | tf_op jit(solution)/shard_map/ppermute | solution.py:20
  80.0 1.6 convert_multiply_fusion.7
  88.5 0.7 fusion.142
  89.2 0.7 add.983
  89.9 0.7 add.996
  90.6 0.6 add.1019
  92.4 0.9 pad.453
  93.7 0.7 add.1021
  94.5 1.0 pad.455
  95.5 0.7 pad_maximum_fusion.3
  96.3 1.0 pad.454
  97.3 0.8 copy-done.6
  98.1 0.8 add.1023
  98.9 4.0 %rev.16 = f32[256,384]{1,0:T(8,128)} reverse(f32[256,384]{1,0:T(8,128)} %add.1023), dimensions={0} | reverse | bytes 786432 | tf_op jit(solution)/shard_map/rev | solution.py:119
  102.8 0.8 add.998
  103.6 3.9 %rev.17 = f32[256,384]{1,0:T(8,128)} reverse(f32[256,384]{1,0:T(8,128)} %add.998), dimensions={0} | reverse | bytes 786432 | tf_op jit(solution)/shard_map/rev | solution.py:119
  107.5 0.7 slice_add_fusion.12
  108.3 13.6 %all-gather.8 = f32[4,4,384]{2,1,0:T(4,128)S(1)} all-gather(f32[1,4,384]{2,1,0:T(4,128)S(1)} %maximum_bitcast_fusion), channel_id=3, replica_groups=mesh['grp'=2,'sp'=4,'tp'=4] {'sp'}, dimensions={0}, use_global_device_ids=true | all-gather | bytes 30720 | tf_op jit(solution)/shard_map/all_gather | solution.py:129
  122.0 20.0 %all-gather.27.cloned.1.call-done = bf16[1,384,2048]{2,1,0:T(8,128)(2,1)} async-done(((bf16[1,384,512]{2,1,0:T(8,128)(2,1)}), bf16[1,384,2048]{2,1,0:T(8,128)(2,1)}) %all-gather.27.cloned.1.call-update) | async-done | bytes 1572880 | tf_op jit(solution)/shard_map/all_gather | solution.py:134
  142.0 4.7 %convolution_convert_fusion.1 = bf16[256,2048]{1,0:T(8,128)(2,1)} fusion(bf16[1,384,2048]{2,1,0:T(8,128)(2,1)} %all-gather.27.cloned.1.call-done, bf16[1,2048,384]{2,1,0:T(8,128)(2,1)} %all-gather.25.cloned.1.call-done, f32[256,384]{1,0:T(8,128)} %rev.17, f32[256,384]{1,0:T(8,128)} %rev.16, f32[256,384]{1,0:T(8,128)S(1)} %pad.422, f32[256,384]{1,0:T(8,128)S(1)} %pad.423, ...), kind=kOutput, calls=%fused_computation.5 | convolution fusion | flops 809795584 | bytes 7614464 | tf_op jit(solution)/shard_map/dot_general | solution.py:132
  146.7 23.7 %reduce-scatter.3.cloned.1.call-done = bf16[256,512]{1,0:T(8,128)(2,1)} async-done(((bf16[256,2048]{1,0:T(8,128)(2,1)}), bf16[256,512]{1,0:T(8,128)(2,1)}) %reduce-scatter.3.cloned.1.call-update) | async-done | bytes 262160 | tf_op jit(solution)/shard_map/reduce_scatter | solution.py:137
  170.5 1.7 add_convert_fusion.1
  172.2 0.7 all-gather.29.cloned.1.call-update
  173.7 0.7 all-gather.33.cloned.1.call-update
  174.5 14.5 %all-gather.21.cloned.1.call-done = bf16[256,2048]{1,0:T(8,128)(2,1)} async-done(((bf16[256,512]{1,0:T(8,128)(2,1)}), bf16[256,2048]{1,0:T(8,128)(2,1)}) %all-gather.21.cloned.1.call-update) | async-done | bytes 1048592 | tf_op jit(solution)/shard_map/all_gather | solution.py:71
  189.0 1.5 fusion.3
  190.6 37.1 %all-gather.29.cloned.1.call-done = bf16[1,2048,384]{2,1,0:T(8,128)(2,1)} async-done(((bf16[1,512,384]{2,1,0:T(8,128)(2,1)}), bf16[1,2048,384]{2,1,0:T(8,128)(2,1)}) %all-gather.29.cloned.1.call-update) | async-done | bytes 1572880 | tf_op jit(solution)/shard_map/all_gather | solution.py:75
  227.7 2.5 fusion.49
  230.2 2.6 collective-permute-start.2
  232.8 1.3 collective-permute-start.3
  234.8 3.6 %collective-permute-done.3 = bf16[2,384]{1,0:T(2,128)(2,1)S(1)} collective-permute-done((bf16[2,384]{1,0:T(2,128)(2,1)S(1)}, bf16[2,384]{1,0:T(2,128)(2,1)S(1)}, u32[]{:S(2)}, u32[]{:S(2)}) %collective-permute-start.3) | collective-permute-done | bytes 1568 | tf_op jit(solution)/shard_map/ppermute | solution.py:20
  240.7 1.6 convert_multiply_fusion.5
  248.6 0.7 fusion.140
  249.3 0.7 add.1077
  250.0 0.6 add.1090
  250.7 0.6 add.1113
  252.5 0.9 pad.517
  253.8 0.7 add.1115
  254.6 1.0 pad.519
  255.6 0.7 pad_maximum_fusion.7
  256.3 1.0 pad.518
  257.4 0.8 copy-done.5
  258.1 0.8 add.1117
  258.9 4.0 %rev.18 = f32[256,384]{1,0:T(8,128)} reverse(f32[256,384]{1,0:T(8,128)} %add.1117), dimensions={0} | reverse | bytes 786432 | tf_op jit(solution)/shard_map/rev | solution.py:119
  262.9 0.8 add.1092
  263.7 3.8 %rev.19 = f32[256,384]{1,0:T(8,128)} reverse(f32[256,384]{1,0:T(8,128)} %add.1092), dimensions={0} | reverse | bytes 786432 | tf_op jit(solution)/shard_map/rev | solution.py:119
  267.5 0.7 slice_add_fusion.2
  268.3 13.5 %all-gather.9 = f32[4,4,384]{2,1,0:T(4,128)S(1)} all-gather(f32[1,4,384]{2,1,0:T(4,128)S(1)} %maximum_bitcast_fusion.1), channel_id=7, replica_groups=mesh['grp'=2,'sp'=4,'tp'=4] {'sp'}, dimensions={0}, use_global_device_ids=true | all-gather | bytes 30720 | tf_op jit(solution)/shard_map/all_gather | solution.py:129
  281.9 20.9 %all-gather.33.cloned.1.call-done = bf16[1,384,2048]{2,1,0:T(8,128)(2,1)} async-done(((bf16[1,384,512]{2,1,0:T(8,128)(2,1)}), bf16[1,384,2048]{2,1,0:T(8,128)(2,1)}) %all-gather.33.cloned.1.call-update) | async-done | bytes 1572880 | tf_op jit(solution)/shard_map/all_gather | solution.py:134
  302.8 4.7 %convolution_convert_fusion = bf16[256,2048]{1,0:T(8,128)(2,1)} fusion(bf16[1,384,2048]{2,1,0:T(8,128)(2,1)} %all-gather.33.cloned.1.call-done, bf16[1,2048,384]{2,1,0:T(8,128)(2,1)} %all-gather.31.cloned.1.call-done, f32[256,384]{1,0:T(8,128)} %rev.19, f32[256,384]{1,0:T(8,128)} %rev.18, f32[256,384]{1,0:T(8,128)S(1)} %pad.486, f32[256,384]{1,0:T(8,128)S(1)} %pad.487, ...), kind=kOutput, calls=%fused_computation.4 | convolution fusion | flops 809795584 | bytes 7614464 | tf_op jit(solution)/shard_map/dot_general | solution.py:132
  307.4 23.8 %reduce-scatter.5.cloned.1.call-done = bf16[256,512]{1,0:T(8,128)(2,1)} async-done(((bf16[256,2048]{1,0:T(8,128)(2,1)}), bf16[256,512]{1,0:T(8,128)(2,1)}) %reduce-scatter.5.cloned.1.call-update) | async-done | bytes 262160 | tf_op jit(solution)/shard_map/reduce_scatter | solution.py:137
  331.2 1.7 add_convert_fusion
  (630 shorter events, 23.1 us)
Async XLA Ops:
  6.5 3.0 copy-start.8
  6.5 21.8 %all-gather.19.cloned.1.call-start = ((), (), s32[]{:S(2)}) async-start(), calls=%async_computation.2 | async-start | bytes 1310720 | tf_op jit(solution)/shard_map/all_gather | solution.py:71
  7.3 59.7 %all-gather.23.cloned.1.call-start = ((), (), s32[]{:S(2)}) async-start(), calls=%async_computation.6 | async-start | bytes 1966080 | tf_op jit(solution)/shard_map/all_gather | solution.py:75
  9.4 1.3 copy-start.9
  9.4 112.5 %all-gather.25.cloned.1.call-start = ((), (), s32[]{:S(2)}) async-start(), calls=%async_computation.7 | async-start | bytes 1966080 | tf_op jit(solution)/shard_map/all_gather | solution.py:80
  10.5 1.3 copy-start.27
  10.5 1.9 copy-start.28
  10.5 2.5 copy-start.31
  10.5 3.1 copy-start.37
  10.5 131.5 %all-gather.27.cloned.1.call-start = ((), (), s32[]{:S(2)}) async-start(), calls=%async_computation.8 | async-start | bytes 1966080 | tf_op jit(solution)/shard_map/all_gather | solution.py:134
  11.7 158.8 %reduce-scatter.3.cloned.1.call-start = ((), (), s32[]{:S(2)}) async-start(), calls=%async_computation.3 | async-start | bytes 1310720 | tf_op jit(solution)/shard_map/reduce_scatter | solution.py:137
  12.4 57.1 %copy-start.18 = (f32[1,2048]{1,0:T(1,128)}, f32[1,2048]{1,0:T(1,128)S(1)}, u32[]{:S(2)}) copy-start(f32[1,2048]{1,0:T(1,128)S(1)} %get-tuple-element.124) | copy-start | bytes 24580
  13.0 64.7 %copy-start.23 = (f32[384]{0:T(512)}, f32[384]{0:T(512)S(1)}, u32[]{:S(2)}) copy-start(f32[384]{0:T(512)S(1)} %get-tuple-element.27) | copy-start | bytes 4612
  13.0 64.7 %copy-start.24 = (f32[384]{0:T(512)}, f32[384]{0:T(512)S(1)}, u32[]{:S(2)}) copy-start(f32[384]{0:T(512)S(1)} %get-tuple-element.28) | copy-start | bytes 4612
  13.0 64.7 %copy-start.25 = (f32[384]{0:T(512)}, f32[384]{0:T(512)S(1)}, u32[]{:S(2)}) copy-start(f32[384]{0:T(512)S(1)} %get-tuple-element.29) | copy-start | bytes 4612
  13.0 64.7 %copy-start.26 = (f32[384]{0:T(512)}, f32[384]{0:T(512)S(1)}, u32[]{:S(2)}) copy-start(f32[384]{0:T(512)S(1)} %get-tuple-element.30) | copy-start | bytes 4612
  29.9 39.6 %copy-start.35 = (f32[256]{0:T(256)}, f32[256]{0:T(256)S(1)}, u32[]{:S(2)}) copy-start(f32[256]{0:T(256)S(1)} %add_rsqrt_fusion.1) | copy-start | bytes 3076
  69.5 8.6 %copy-start.38 = (bf16[2,2,2,3,128,128]{5,4,3,2,1,0:T(8,128)(2,1)S(1)}, bf16[2,2,2,3,128,128]{5,4,3,2,1,0:T(8,128)(2,1)}, u32[]{:S(2)}) copy-start(bf16[2,2,2,3,128,128]{5,4,3,2,1,0:T(8,128)(2,1)} %param.15) | copy-start | bytes 2359300
  69.5 4.5 %collective-permute-start = (bf16[2,384]{1,0:T(2,128)(2,1)S(1)}, bf16[2,384]{1,0:T(2,128)(2,1)S(1)}, u32[]{:S(2)}, u32[]{:S(2)}) collective-permute-start(bf16[2,384]{1,0:T(2,128)(2,1)S(1)} %get-tuple-element.73), channel_id=1, source_target_pairs={{0,4},{4,8},{8,12},{1,5},{5,9},{9,13},{2,6},{6,10},{10,14},{3,7},{... | collective-permute-start | bytes 4616 | tf_op jit(solution)/shard_map/ppermute | solution.py:18
  72.1 5.5 %collective-permute-start.1 = (bf16[2,384]{1,0:T(2,128)(2,1)S(1)}, bf16[2,384]{1,0:T(2,128)(2,1)S(1)}, u32[]{:S(2)}, u32[]{:S(2)}) collective-permute-start(bf16[2,384]{1,0:T(2,128)(2,1)S(1)} %get-tuple-element.74), channel_id=1, source_target_pairs={{4,0},{8,4},{12,8},{5,1},{9,5},{13,9},{6,2},{10,6},{14,10},{7,3},{... | collective-permute-start | bytes 4616 | tf_op jit(solution)/shard_map/ppermute | solution.py:20
  87.5 0.7 copy-start.32
  89.9 1.6 copy-start.10
  91.2 0.9 copy-start.12
  91.3 0.9 copy-start.14
  95.5 1.8 copy-start.4
  97.3 0.8 copy-start.6
  98.9 43.1 %copy-start = (bf16[256,2048]{1,0:T(8,128)(2,1)S(1)}, bf16[256,2048]{1,0:T(8,128)(2,1)}, u32[]{:S(2)}) copy-start(bf16[256,2048]{1,0:T(8,128)(2,1)} %all-gather.19.cloned.1.call-done) | copy-start | bytes 3145732
  98.9 43.1 %copy-start.19 = (f32[1,2048]{1,0:T(1,128)S(1)}, f32[1,2048]{1,0:T(1,128)}, u32[]{:S(2)}) copy-start(f32[1,2048]{1,0:T(1,128)} %copy-done.18) | copy-start | bytes 24580
  98.9 43.1 %copy-start.36 = (f32[256]{0:T(256)S(1)}, f32[256]{0:T(256)}, u32[]{:S(2)}) copy-start(f32[256]{0:T(256)} %copy-done.35) | copy-start | bytes 3076
  121.9 48.5 %copy-start.7 = (bf16[256,512]{1,0:T(8,128)(2,1)S(1)}, bf16[256,512]{1,0:T(8,128)(2,1)}, u32[]{:S(2)}) copy-start(bf16[256,512]{1,0:T(8,128)(2,1)} %param.9) | copy-start | bytes 786436
  146.7 81.0 %copy-start.16 = (f32[1,2048]{1,0:T(1,128)S(1)}, f32[1,2048]{1,0:T(1,128)}, u32[]{:S(2)}) copy-start(f32[1,2048]{1,0:T(1,128)} %get-tuple-element.123) | copy-start | bytes 24580
  146.7 42.3 %all-gather.21.cloned.1.call-start = ((), (), s32[]{:S(2)}) async-start(), calls=%async_computation.4 | async-start | bytes 1310720 | tf_op jit(solution)/shard_map/all_gather | solution.py:71
  172.2 55.5 %all-gather.29.cloned.1.call-start = ((), (), s32[]{:S(2)}) async-start(), calls=%async_computation.9 | async-start | bytes 1966080 | tf_op jit(solution)/shard_map/all_gather | solution.py:75
  172.9 108.9 %all-gather.31.cloned.1.call-start = ((), (), s32[]{:S(2)}) async-start(), calls=%async_computation.10 | async-start | bytes 1966080 | tf_op jit(solution)/shard_map/all_gather | solution.py:80
  173.7 129.1 %all-gather.33.cloned.1.call-start = ((), (), s32[]{:S(2)}) async-start(), calls=%async_computation.11 | async-start | bytes 1966080 | tf_op jit(solution)/shard_map/all_gather | solution.py:134
  174.4 156.8 %reduce-scatter.5.cloned.1.call-start = ((), (), s32[]{:S(2)}) async-start(), calls=%async_computation.5 | async-start | bytes 1310720 | tf_op jit(solution)/shard_map/reduce_scatter | solution.py:137
  190.5 39.6 %copy-start.33 = (f32[256]{0:T(256)}, f32[256]{0:T(256)S(1)}, u32[]{:S(2)}) copy-start(f32[256]{0:T(256)S(1)} %add_rsqrt_fusion) | copy-start | bytes 3076
  227.7 6.5 %copy-start.29 = (f32[384]{0:T(512)S(1)}, f32[384]{0:T(512)}, u32[]{:S(2)}) copy-start(f32[384]{0:T(512)} %get-tuple-element.33) | copy-start | bytes 4612
  227.7 6.5 %copy-start.30 = (f32[384]{0:T(512)S(1)}, f32[384]{0:T(512)}, u32[]{:S(2)}) copy-start(f32[384]{0:T(512)} %get-tuple-element.36) | copy-start | bytes 4612
  227.7 10.7 %copy-start.20 = (f32[384]{0:T(512)S(1)}, f32[384]{0:T(512)}, u32[]{:S(2)}) copy-start(f32[384]{0:T(512)} %get-tuple-element.26) | copy-start | bytes 4612
  227.7 10.7 %copy-start.21 = (f32[384]{0:T(512)S(1)}, f32[384]{0:T(512)}, u32[]{:S(2)}) copy-start(f32[384]{0:T(512)} %get-tuple-element.31) | copy-start | bytes 4612
  227.7 10.7 %copy-start.22 = (f32[384]{0:T(512)S(1)}, f32[384]{0:T(512)}, u32[]{:S(2)}) copy-start(f32[384]{0:T(512)} %get-tuple-element.32) | copy-start | bytes 4612
  230.2 8.6 %copy-start.39 = (bf16[2,2,2,3,128,128]{5,4,3,2,1,0:T(8,128)(2,1)S(1)}, bf16[2,2,2,3,128,128]{5,4,3,2,1,0:T(8,128)(2,1)}, u32[]{:S(2)}) copy-start(bf16[2,2,2,3,128,128]{5,4,3,2,1,0:T(8,128)(2,1)} %param.15) | copy-start | bytes 2359300
  230.2 4.6 %collective-permute-start.2 = (bf16[2,384]{1,0:T(2,128)(2,1)S(1)}, bf16[2,384]{1,0:T(2,128)(2,1)S(1)}, u32[]{:S(2)}, u32[]{:S(2)}) collective-permute-start(bf16[2,384]{1,0:T(2,128)(2,1)S(1)} %get-tuple-element.61), channel_id=1, source_target_pairs={{0,4},{4,8},{8,12},{1,5},{5,9},{9,13},{2,6},{6,10},{10,14},{3,7},{... | collective-permute-start | bytes 4616 | tf_op jit(solution)/shard_map/ppermute | solution.py:18
  232.8 5.5 %collective-permute-start.3 = (bf16[2,384]{1,0:T(2,128)(2,1)S(1)}, bf16[2,384]{1,0:T(2,128)(2,1)S(1)}, u32[]{:S(2)}, u32[]{:S(2)}) collective-permute-start(bf16[2,384]{1,0:T(2,128)(2,1)S(1)} %get-tuple-element.62), channel_id=1, source_target_pairs={{4,0},{8,4},{12,8},{5,1},{9,5},{13,9},{6,2},{10,6},{14,10},{7,3},{... | collective-permute-start | bytes 4616 | tf_op jit(solution)/shard_map/ppermute | solution.py:20
  250.0 1.6 copy-start.11
  251.3 0.9 copy-start.13
  251.4 0.9 copy-start.15
  255.6 1.8 copy-start.3
  257.4 0.8 copy-start.5
  258.9 43.8 %copy-start.1 = (bf16[256,2048]{1,0:T(8,128)(2,1)S(1)}, bf16[256,2048]{1,0:T(8,128)(2,1)}, u32[]{:S(2)}) copy-start(bf16[256,2048]{1,0:T(8,128)(2,1)} %all-gather.21.cloned.1.call-done) | copy-start | bytes 3145732
  258.9 43.8 %copy-start.17 = (f32[1,2048]{1,0:T(1,128)S(1)}, f32[1,2048]{1,0:T(1,128)}, u32[]{:S(2)}) copy-start(f32[1,2048]{1,0:T(1,128)} %get-tuple-element.123) | copy-start | bytes 24580
  258.9 43.8 %copy-start.34 = (f32[256]{0:T(256)S(1)}, f32[256]{0:T(256)}, u32[]{:S(2)}) copy-start(f32[256]{0:T(256)} %copy-done.33) | copy-start | bytes 3076
  281.9 49.4 %copy-start.2 = (bf16[256,512]{1,0:T(8,128)(2,1)S(1)}, bf16[256,512]{1,0:T(8,128)(2,1)}, u32[]{:S(2)}) copy-start(bf16[256,512]{1,0:T(8,128)(2,1)} %add_convert_fusion.1) | copy-start | bytes 786436
Sparse Core Ops, SparseCore 0:
  8.9 19.4 all-gather.18
  29.9 37.0 all-gather.22
  68.5 35.8 all-gather.24
  105.9 36.0 all-gather.26
  146.8 23.6 reduce-scatter.2
  172.3 16.6 all-gather.20
  190.6 37.0 all-gather.28
  229.2 35.8 all-gather.30
  266.7 35.9 all-gather.32
  307.6 23.6 reduce-scatter.4

commit v2 on v1

v2 whole, which is shorter than its diff:
```python
import functools

import jax
import jax.numpy as jnp
from jax import lax
from jax.experimental import pallas as pl
from jax.experimental.pallas import tpu as pltpu
from jax.sharding import PartitionSpec as P

EPS = 1e-06
RECURRENT_WIDTH = 8.0
TILE = 16
HALO = 8
MESH = pl.DeviceIdType.MESH


def own_share(rows, n_grp):
    if n_grp != 2:
        return rows
    return min(rows, -(-rows * 3 // (5 * TILE)) * TILE)


def one_minus_square(log_decay, decay):
    y = 2.0 * log_decay
    series = y * (1 / 720) + 1 / 120
    series = series * y + 1 / 24
    series = series * y + 1 / 6
    series = series * y + 0.5
    series = series * y + 1.0
    return jnp.where(y > -0.25, -y * series, 1.0 - decay * decay)


def scanned(a, b, reverse):
    count = a.shape[0]
    row = lax.broadcasted_iota(jnp.int32, a.shape, 0)
    step = 1
    while step < count:
        inside = row < count - step if reverse else row >= step
        shift = count - step if reverse else step
        a_near = jnp.where(inside, pltpu.roll(a, shift, 0), 1.0)
        b_near = jnp.where(inside, pltpu.roll(b, shift, 0), 0.0)
        b = a * b_near + b
        a = a * a_near
        step *= 2
    return a, b


def kernel(
    n_grp, n_sp, n_tp,
    stream, gain, conv_w, gate_w, out_w, taps, blocks, rate, boost,
    out,
    full, normed, g_in, g_out, xpad, y_act, cum, loc, ends, gated, parts, sums,
    z_send, z_recv, y_send, y_recv, f_send, f_recv, r_send, r_recv,
    h_send, h_recv, e_send, e_recv,
):
    g, s, t = lax.axis_index("grp"), lax.axis_index("sp"), lax.axis_index("tp")
    layers = conv_w.shape[0]
    rows, ds = stream.shape
    cs, channels = conv_w.shape[1], conv_w.shape[2]
    width = blocks.shape[-1]
    weights = 3 * layers

    def remote(src, dst, send, recv, axis, place):
        return pltpu.make_async_remote_copy(
            src_ref=src, dst_ref=dst, send_sem=send, recv_sem=recv,
            device_id={axis: place}, device_id_type=MESH,
        )

    barrier = pltpu.get_barrier_semaphore()
    total = 0
    for axis, me, count in (("sp", s, n_sp), ("tp", t, n_tp), ("grp", g, n_grp)):
        for d in range(1, count):
            pl.semaphore_signal(
                barrier, inc=1, device_id={axis: lax.rem(me + d, count)}, device_id_type=MESH
            )
            total += 1
    pl.semaphore_wait(barrier, total)

    def mine(w):
        return (conv_w, gate_w, out_w)[w % 3].at[w // 3]

    def hold(w, c):
        return g_out.at[w // 3, c] if w % 3 == 2 else g_in.at[w // 3 * 2 + w % 3, c]

    def depth(w):
        return channels if w % 3 == 2 else cs

    def z_rows(w):
        share = own_share(depth(w), n_grp)
        if share == depth(w):
            return pl.ds(0, share)
        return pl.ds(pl.multiple_of(g * (depth(w) - share), TILE), share)

    def y_rows(w, place):
        share = own_share(depth(w), n_grp)
        return pl.ds(pl.multiple_of(place * share, TILE), depth(w) - share)

    def z_copy(w, c, src, to, slot):
        return remote(
            src.at[z_rows(w)], hold(w, c).at[z_rows(w)],
            z_send.at[w, slot], z_recv.at[w, c], "sp", to,
        )

    shared = n_grp == 2

    def y_copy(w, c, place):
        return remote(
            hold(w, c).at[y_rows(w, place)], hold(w, c).at[y_rows(w, place)],
            y_send.at[w, c], y_recv.at[w, c], "grp", 1 - g,
        )

    def has_y(w):
        return shared and own_share(depth(w), n_grp) < depth(w)

    def start_own(w):
        @pl.when(s < n_sp - 1)
        def _():
            z_copy(w, s, mine(w), s + 1, s).start()

        @pl.when(s > 0)
        def _():
            z_copy(w, s, mine(w), s - 1, n_sp).start()

    def pass_on(w, c, onward, to, back):
        z_copy(w, c, hold(w, c), back, c).wait_recv()

        @pl.when(onward)
        def _():
            z_copy(w, c, hold(w, c), to, c).start()

        if has_y(w):
            y_copy(w, c, g).start()

    def event(w, k):
        @pl.when(s - 1 - k >= 0)
        def _():
            pass_on(w, s - 1 - k, s < n_sp - 1, s + 1, s - 1)

        @pl.when(s + 1 + k <= n_sp - 1)
        def _():
            pass_on(w, s + 1 + k, s > 0, s - 1, s + 1)

        if k == 0 and w + 2 < weights:
            start_own(w + 2)

    queue = [(w, k) for w in range(weights) for k in range(n_sp - 1)]

    def serve(count):
        for _ in range(min(count, len(queue))):
            event(*queue.pop(0))

    def serve_until(w):
        while queue and queue[0][0] <= w:
            event(*queue.pop(0))

    def landed(w):
        if has_y(w):
            for c in range(n_sp):
                @pl.when(c != s)
                def _():
                    y_copy(w, c, 1 - g).wait_recv()

    def f_copy(layer, src, source, d, to):
        return remote(
            src, full.at[layer, source], f_send.at[layer, d], f_recv.at[layer, source], "tp", to
        )

    tp_order = [d for d in range(1, n_tp)]

    def send_features(layer, src):
        for d in tp_order:
            f_copy(layer, src, t, d, lax.rem(t + d, n_tp)).start()

    send_features(0, stream)
    for w in range(min(2, weights)):
        start_own(w)
    full[0, t] = stream[...]
    for w in range(weights):
        if w % 3 == 2:
            g_out[w // 3, s] = out_w[w // 3]
        else:
            g_in[w // 3 * 2 + w % 3, s] = (conv_w, gate_w)[w % 3][w // 3]

    row = lax.broadcasted_iota(jnp.int32, (rows, 1), 0)

    for layer in range(layers):
        if layer == 0:
            serve(1)
        for d in tp_order:
            source = lax.rem(t + d, n_tp)
            f_copy(layer, full.at[layer, source], source, d, source).wait_recv()
        square = jnp.zeros((rows, 1), jnp.float32)
        for j in range(n_tp):
            x = full[layer, j].astype(jnp.float32)
            square += jnp.sum(x * x, axis=-1, keepdims=True)
        inverse = lax.rsqrt(square / (n_tp * ds) + EPS)
        piece = min(cs, ds)
        for p in range(n_tp * ds // piece):
            at = p * piece
            x = full[layer, at // ds, :, at % ds : at % ds + piece].astype(jnp.float32)
            x = x * inverse * gain[layer : layer + 1, at : at + piece]
            normed[at // cs, :, at % cs : at % cs + piece] = x.astype(jnp.bfloat16)

        def project(w):
            acc = None
            for c in range(n_sp):
                term = jnp.dot(
                    normed[c], g_in[w // 3 * 2 + w % 3, c], preferred_element_type=jnp.float32
                )
                acc = term if acc is None else acc + term
            return acc.astype(jnp.bfloat16).astype(jnp.float32)

        wx, wy, wo = 3 * layer, 3 * layer + 1, 3 * layer + 2
        serve_until(wx)
        if layer == 0:
            serve(1)
        landed(wx)
        xpad[layer, HALO : HALO + rows] = project(wx)

        def halo_right():
            return remote(
                xpad.at[layer, pl.ds(rows, HALO)], xpad.at[layer, pl.ds(0, HALO)],
                h_send.at[layer, 0], h_recv.at[layer, 0], "sp", lax.rem(s + 1, n_sp),
            )

        def halo_left():
            return remote(
                xpad.at[layer, pl.ds(HALO, HALO)], xpad.at[layer, pl.ds(HALO + rows, HALO)],
                h_send.at[layer, 1], h_recv.at[layer, 1], "sp", lax.rem(s + n_sp - 1, n_sp),
            )

        @pl.when(s < n_sp - 1)
        def _():
            halo_right().start()

        @pl.when(s > 0)
        def _():
            halo_left().start()

        serve_until(wy)
        landed(wy)
        y_act[...] = jax.nn.gelu(project(wy))

        @pl.when(s > 0)
        def _():
            halo_right().wait_recv()

        @pl.when(s == 0)
        def _():
            xpad[layer, 0:HALO] = jnp.zeros((HALO, channels), jnp.float32)

        @pl.when(s < n_sp - 1)
        def _():
            halo_left().wait_recv()

        @pl.when(s == n_sp - 1)
        def _():
            xpad[layer, HALO + rows : 2 * HALO + rows] = jnp.zeros((HALO, channels), jnp.float32)

        for n in range(channels // width):
            lanes = slice(n * width, (n + 1) * width)
            conv = None
            for k in range(taps.shape[1]):
                term = taps[layer, k : k + 1, lanes] * xpad[
                    layer, HALO - 1 + k : HALO - 1 + k + rows, lanes
                ]
                conv = term if conv is None else conv + term
            conv_half = conv.astype(jnp.bfloat16)
            conv = conv_half.astype(jnp.float32)
            for d in range(2):
                recur = jax.nn.sigmoid(
                    jnp.dot(conv_half, blocks[layer, d, 0, n], preferred_element_type=jnp.float32)
                )
                inject = jax.nn.sigmoid(
                    jnp.dot(conv_half, blocks[layer, d, 1, n], preferred_element_type=jnp.float32)
                )
                at = 2 * layer + d
                log_decay = rate[at : at + 1, lanes] * recur + boost[:, at : at + 1]
                decay = jnp.exp(log_decay)
                first = (row == 0) & (s == 0) if d == 0 else (row == rows - 1) & (s == n_sp - 1)
                m = jnp.where(first, 1.0, jnp.sqrt(one_minus_square(log_decay, decay)))
                a, b = scanned(decay, m * inject * conv, d == 1)
                cum[d, :, lanes] = a
                loc[d, :, lanes] = b
                edge = rows - 1 if d == 0 else 0
                ends[layer, s, 2 * d : 2 * d + 1, lanes] = a[edge : edge + 1]
                ends[layer, s, 2 * d + 1 : 2 * d + 2, lanes] = b[edge : edge + 1]
            serve(1)

        def e_copy(source, d, to):
            return remote(
                ends.at[layer, source], ends.at[layer, source],
                e_send.at[layer, d], e_recv.at[layer, source], "sp", to,
            )

        for d in range(1, n_sp):
            e_copy(s, d, lax.rem(s + d, n_sp)).start()
        serve_until(wo)
        for d in range(1, n_sp):
            source = lax.rem(s + d, n_sp)
            e_copy(source, d, source).wait_recv()
        forward = jnp.zeros((1, channels), jnp.float32)
        backward = forward
        for step in range(n_sp - 1):
            forward = jnp.where(
                step < s, ends[layer, step, 0:1] * forward + ends[layer, step, 1:2], forward
            )
            back = n_sp - 1 - step
            backward = jnp.where(
                back > s, ends[layer, back, 2:3] * backward + ends[layer, back, 3:4], backward
            )
        state = loc[0] + cum[0] * forward + loc[1] + cum[1] * backward
        gated[...] = (state * y_act[...]).astype(jnp.bfloat16)

        def r_copy(source, slot, to):
            return remote(
                parts.at[layer, to], sums.at[layer, source],
                r_send.at[layer, slot], r_recv.at[layer, source], "tp", to,
            )

        landed(wo)
        for c in range(n_sp):
            partial = jnp.dot(gated[...], g_out[layer, c], preferred_element_type=jnp.float32)
            partial = partial.astype(jnp.bfloat16)
            for q in range(cs // piece):
                at = c * cs + q * piece
                j = at // ds
                parts[layer, j, :, at % ds : at % ds + piece] = partial[
                    :, q * piece : (q + 1) * piece
                ]
                if (at + piece) % ds == 0:
                    @pl.when(j != t)
                    def _():
                        r_copy(t, j, j).start()

        if layer == 0:
            serve(n_sp - 1)
        new = full[layer, t].astype(jnp.float32) + parts[layer, t].astype(jnp.float32)
        for d in tp_order:
            source = lax.rem(t + d, n_tp)
            r_copy(source, source, source).wait_recv()
            new = new + sums[layer, source].astype(jnp.float32)
        new = new.astype(jnp.bfloat16)
        if layer + 1 < layers:
            full[layer + 1, t] = new
            send_features(layer + 1, full.at[layer + 1, t])
        else:
            out[...] = new

    for w in range(weights):
        @pl.when(s < n_sp - 1)
        def _():
            z_copy(w, s, mine(w), s + 1, s).wait_send()

        @pl.when(s > 0)
        def _():
            z_copy(w, s, mine(w), s - 1, n_sp).wait_send()

        for c in range(n_sp):
            @pl.when(((c < s) & (s < n_sp - 1)) | ((c > s) & (s > 0)))
            def _():
                z_copy(w, c, hold(w, c), lax.rem(s + 1, n_sp), c).wait_send()

            if has_y(w):
                @pl.when(c != s)
                def _():
                    y_copy(w, c, g).wait_send()

    for layer in range(layers):
        for d in tp_order:
            f_copy(layer, full.at[layer, t], t, d, lax.rem(t + d, n_tp)).wait_send()
        for j in range(n_tp):
            @pl.when(j != t)
            def _():
                remote(
                    parts.at[layer, j], sums.at[layer, t],
                    r_send.at[layer, j], r_recv.at[layer, t], "tp", j,
                ).wait_send()

        for d in range(1, n_sp):
            remote(
                ends.at[layer, s], ends.at[layer, s],
                e_send.at[layer, d], e_recv.at[layer, s], "sp", lax.rem(s + d, n_sp),
            ).wait_send()

        @pl.when(s < n_sp - 1)
        def _():
            remote(
                xpad.at[layer, pl.ds(rows, HALO)], xpad.at[layer, pl.ds(0, HALO)],
                h_send.at[layer, 0], h_recv.at[layer, 0], "sp", lax.rem(s + 1, n_sp),
            ).wait_send()

        @pl.when(s > 0)
        def _():
            remote(
                xpad.at[layer, pl.ds(HALO, HALO)], xpad.at[layer, pl.ds(HALO + rows, HALO)],
                h_send.at[layer, 1], h_recv.at[layer, 1], "sp", lax.rem(s + n_sp - 1, n_sp),
            ).wait_send()


def solution(mesh):
    n_grp, n_sp, n_tp = mesh.shape["grp"], mesh.shape["sp"], mesh.shape["tp"]

    def local(stream, gain, conv_w, gate_w, out_w, taps, blocks, logit, boost):
        layers, cs, channels = conv_w.shape
        rows, ds = stream.shape
        rate = (-RECURRENT_WIDTH * jax.nn.softplus(-logit)).reshape(-1, channels)
        boost = boost.reshape(-1, rows).T
        bf, f32, dma = jnp.bfloat16, jnp.float32, pltpu.SemaphoreType.DMA
        vmem = pltpu.VMEM
        return pl.pallas_call(
            functools.partial(kernel, n_grp, n_sp, n_tp),
            out_shape=jax.ShapeDtypeStruct((rows, ds), bf),
            in_specs=[pl.BlockSpec(memory_space=vmem)] * 9,
            out_specs=pl.BlockSpec(memory_space=vmem),
            scratch_shapes=[
                vmem((layers, n_tp, rows, ds), bf),
                vmem((n_sp, rows, cs), bf),
                vmem((2 * layers, n_sp, cs, channels), bf),
                vmem((layers, n_sp, channels, cs), bf),
                vmem((layers, rows + 2 * HALO, channels), f32),
                vmem((rows, channels), f32),
                vmem((2, rows, channels), f32),
                vmem((2, rows, channels), f32),
                vmem((layers, n_sp, 8, channels), f32),
                vmem((rows, channels), bf),
                vmem((layers, n_tp, rows, ds), bf),
                vmem((layers, n_tp, rows, ds), bf),
                dma((3 * layers, n_sp + 1)),
                dma((3 * layers, n_sp)),
                dma((3 * layers, n_sp)),
                dma((3 * layers, n_sp)),
                dma((layers, n_tp)),
                dma((layers, n_tp)),
                dma((layers, n_tp)),
                dma((layers, n_tp)),
                dma((layers, 2)),
                dma((layers, 2)),
                dma((layers, n_sp)),
                dma((layers, n_sp)),
            ],
            compiler_params=pltpu.CompilerParams(
                collective_id=0, has_side_effects=True, vmem_limit_bytes=60 * 1024 * 1024
            ),
        )(stream, gain, conv_w, gate_w, out_w, taps, blocks, rate, boost)

    return jax.shard_map(
        local,
        mesh=mesh,
        in_specs=(
            P(("grp", "sp"), "tp"),
            P(),
            P(None, "sp", "tp"),
            P(None, "sp", "tp"),
            P(None, "tp", "sp"),
            P(None, None, "tp"),
            P(None, None, None, "tp", None, None),
            P(None, None, "tp"),
            P(None, None, ("grp", "sp")),
        ),
        out_specs=P(("grp", "sp"), "tp"),
        check_vma=False,
    )
```

time: 341 us -> 143 us (0.42)
  waiting for transfers between devices: 201 us -> 0 us
  Pallas kernels: 0 us -> 138 us
  local copies, waits for them, and re-layouts: 42.5 us -> 3.8 us
  other arithmetic: 27.8 us -> 0.02 us
  blocking collectives: 27 us -> 0 us
  between operations: 16.9 us -> 0.02 us
  matrix products: 16.7 us -> 0 us
  starting transfers between devices: 8.38 us -> 0 us
    all_gather x8 -> x0, waiting for transfers between devices: 143 us -> none  [the longest x2 74.2 us: local(): lax.all_gather(convolution_in_weight[layer_index], 'sp', axis=0, tiled=True)]
    pallas_call x0 -> x1, Pallas kernels: none -> 138 us  [local(): pl.pallas_call(functools.partial(kernel, n_grp, n_sp, n_tp), out_shape=ja...]
    reduce_scatter x2 -> x0, waiting for transfers between devices: 47.5 us -> none  [local(): lax.psum_scatter(partials.astype(jnp.float32).astype(jnp.bfloat16), 'tp',...]
    all_gather x2 -> x0, blocking collectives: 27 us -> none  [local(): lax.all_gather(ends, 'sp')]
    dot_general x12 -> x0, matrix products: 16.7 us -> none  [the longest x2 9.31 us: local(): jnp.dot(gated, lax.all_gather(output_weight[layer_index], 'sp', axis=1, t...]
    rev x4 -> x0, local copies, waits for them, and re-layouts: 15.6 us -> none  [local(): lax.associative_scan(combine_pairs, (jnp.exp(decay_logarithm), driven), r...]
    slice x228 -> x0, local copies, waits for them, and re-layouts: 14.7 us -> none  [the longest x220 8.85 us: local(): lax.associative_scan(combine_pairs, (jnp.exp(decay_logarithm), driven), r...]
    add x120 -> x0, other arithmetic: 12.8 us -> none  [the longest x68 10.5 us: local(): lax.associative_scan(combine_pairs, (jnp.exp(decay_logarithm), driven), r...]
  transfers between devices with their start and end apart: 14 -> 0, of which waited for: 10 -> 0; matrix products, arithmetic and copies ran while one was open for 21% -> 0% of each run, Pallas kernels for 0% -> 0%
where the time goes in v2:
time: 143 us; the launch traced here: 142 us
  Pallas kernels  138 us (97%)
  local copies, waits for them, and re-layouts  3.8 us (3%)
    pallas_call x1, Pallas kernels, local(): pl.pallas_call(functools.partial(kernel, n_grp, n_sp, n_tp), out_shape=ja...  138 us

profile of v2, /device:TPU:0, one launch (start us, length us, event | category | flops | bytes accessed | tf_op | source)
XLA Modules:
  0.0 141.6 jit_solution(2675685367544811200)
XLA Ops:
  0.0 0.0 copy-start
  0.0 0.7 reshape.7
  0.7 0.0 copy-done
  0.7 0.6 reshape.6.rate
  1.4 0.8 copy.11
  2.2 137.7 %shard_map.91 = bf16[256,512]{1,0:T(8,128)(2,1)} custom-call(bf16[256,512]{1,0:T(8,128)(2,1)} %stream.1, f32[2,2048]{1,0:T(2,128)} %gain.1, bf16[2,512,384]{2,1,0:T(8,128)(2,1)} %conv_w.1, bf16[2,512,384]{2,1,0:T(8,128)(2,1)} %gate_w.1, bf16[2,384,512]{2,1,0:T(8,128)(2,1)} %out_w.1, f32[2,4,384]{2,1,0:T(4,128)} %taps.1, ...), custom_call_target="tpu_custom_call" | custom-call | tf_op jit(solution)/shard_map/pallas_call | solution.py:411
  139.9 1.7 %copy.13 = bf16[256,512]{1,0:T(8,128)(2,1)} copy(bf16[256,512]{1,0:T(8,128)(2,1)} %shard_map.91) | data formatting | bytes 524288
  (1 shorter events, 0.0 us)
Async XLA Ops:
  0.0 0.7 copy-start

commit v3 on v2

--- a/solution.py
+++ b/solution.py
@@ -17,7 +17,7 @@
 def own_share(rows, n_grp):
     if n_grp != 2:
         return rows
-    return min(rows, -(-rows * 3 // (5 * TILE)) * TILE)
+    return min(rows, -(-rows * 11 // (20 * TILE)) * TILE)
 
 
 def one_minus_square(log_decay, decay):

time: 143 us -> 138 us (0.965); the launches traced: 142 us -> 138 us
  Pallas kernels: 138 us -> 134 us
    pallas_call x1, Pallas kernels: 138 us -> 134 us  [local(): pl.pallas_call(functools.partial(kernel, n_grp, n_sp, n_tp), out_shape=ja...]
where the time goes in v3:
time: 138 us
  Pallas kernels  134 us (97%)
  local copies, waits for them, and re-layouts  3.8 us (3%)
    pallas_call x1, Pallas kernels, local(): pl.pallas_call(functools.partial(kernel, n_grp, n_sp, n_tp), out_shape=ja...  134 us

profile of v3, /device:TPU:0, one launch (start us, length us, event | category | flops | bytes accessed | tf_op | source)
XLA Modules:
  0.0 138.1 jit_solution(18310073384874064984)
XLA Ops:
  0.0 0.0 copy-start
  0.0 0.7 reshape.7
  0.7 0.0 copy-done
  0.7 0.6 reshape.6.rate
  1.4 0.8 copy.11
  2.2 134.2 %shard_map.91 = bf16[256,512]{1,0:T(8,128)(2,1)} custom-call(bf16[256,512]{1,0:T(8,128)(2,1)} %stream.1, f32[2,2048]{1,0:T(2,128)} %gain.1, bf16[2,512,384]{2,1,0:T(8,128)(2,1)} %conv_w.1, bf16[2,512,384]{2,1,0:T(8,128)(2,1)} %gate_w.1, bf16[2,384,512]{2,1,0:T(8,128)(2,1)} %out_w.1, f32[2,4,384]{2,1,0:T(4,128)} %taps.1, ...), custom_call_target="tpu_custom_call" | custom-call | tf_op jit(solution)/shard_map/pallas_call | solution.py:411
  136.4 1.7 %copy.13 = bf16[256,512]{1,0:T(8,128)(2,1)} copy(bf16[256,512]{1,0:T(8,128)(2,1)} %shard_map.91) | data formatting | bytes 524288
  (1 shorter events, 0.0 us)
Async XLA Ops:
  0.0 0.7 copy-start
